TPU v7x, 32 devices: a whole 2x2x4 slice. The times are simulated.
32 devices in a mesh: sp: 8 (over z, y), dp: 4 (over x, core).
Axes of the slice: x: 2, y: 2, z: 4, core: 2. Of those that a mesh axis runs over, the one named last changes fastest.
Arguments:
- query: bfloat16 [4, 1536, 3072], P('dp', 'sp'), may hold values from -18 to 18
- latent: bfloat16 [4, 1536, 1024], P('dp', 'sp'), may hold values from -6 to 6
- rope_key: bfloat16 [4, 1536, 32], P('dp', 'sp'), may hold values from -5 to 5
- latent_norm_gain: float32 [1024], replicated, may hold values from 0.1 to 1.9
- key_up_matrix: bfloat16 [2048, 1024], P('dp'), may hold values from -0.1875 to 0.1875
- value_up_matrix: bfloat16 [2048, 1024], P('dp'), may hold values from -0.1875 to 0.1875
- out_grad: bfloat16 [4, 1536, 2048], P('dp', 'sp'), may hold values from -6 to 6
Outputs:
- query_grad: bfloat16 [4, 1536, 3072], P('dp', 'sp')
- latent_grad: float32 [4, 1536, 1024], P('dp', 'sp')
- rope_key_grad: float32 [4, 1536, 32], P('dp', 'sp')
- key_weight_grad: float32 [2048, 1024], P('dp')
- value_weight_grad: float32 [2048, 1024], P('dp')
- gain_grad: float32 [1024], replicated
All inputs are finite; a program needn't handle non-finite values.
Results may differ from a plain program's by a relative error of at most 0.011.
Values may be sent and summed in bfloat16 or wider, within the bound.
A program may use at most 256 MiB of HBM per device.

v0:
```python
import jax
import jax.numpy as jnp
from jax import lax
from jax.sharding import PartitionSpec as P

ATTENTION_HEADS = 32
PLAIN_HEAD_WIDTH = 64
ROPE = 32
VALUE_HEAD_WIDTH = 64
SPAN = 64
eps = 1e-06
rope_base = 10000.0


def rotate(values, cosine, sine):
    half = values.shape[-1] // 2
    first = values[..., :half]
    second = values[..., half:]
    return jnp.concatenate(
        [first * cosine - second * sine, second * cosine + first * sine], axis=-1
    )


def angles(length, width):
    inverse = 1.0 / rope_base ** (jnp.arange(0, width, 2, dtype=jnp.float32) / width)
    turned = jnp.arange(length, dtype=jnp.float32)[:, None] * inverse[None, :]
    return (jnp.cos(turned), jnp.sin(turned))


def attend_backward(arrived, rope_full):
    f32 = jnp.float32
    bf16 = jnp.bfloat16
    length = arrived.shape[0]
    local_heads = arrived.shape[1]
    width = PLAIN_HEAD_WIDTH + ROPE
    scale = width ** (-0.5)
    block = 512
    cosine, sine = angles(length, ROPE)
    neg = jnp.finfo(f32).min
    q_nope = arrived[:, :, :PLAIN_HEAD_WIDTH]
    q_rope = rotate(
        arrived[:, :, PLAIN_HEAD_WIDTH:width].astype(f32), cosine[:, None, :], sine[:, None, :]
    ).astype(bf16)
    key_nope = arrived[:, :, width : width + PLAIN_HEAD_WIDTH]
    values = arrived[:, :, width + PLAIN_HEAD_WIDTH : width + PLAIN_HEAD_WIDTH + VALUE_HEAD_WIDTH]
    d_out = arrived[:, :, width + PLAIN_HEAD_WIDTH + VALUE_HEAD_WIDTH :]
    k_rope = rotate(rope_full.astype(f32), cosine, sine).astype(bf16)
    dk_nope = jnp.zeros((length, local_heads, PLAIN_HEAD_WIDTH), f32)
    dk_rope = jnp.zeros((length, ROPE), f32)
    d_vals = jnp.zeros((length, local_heads, VALUE_HEAD_WIDTH), f32)
    dq_parts = []
    for begin in range(0, length, block):
        end = begin + block
        qn = q_nope[begin:end]
        qr = q_rope[begin:end]
        go = d_out[begin:end]
        scores = jnp.einsum("qhd,khd->hqk", qn, key_nope[:end], preferred_element_type=f32)
        scores = (
            scores + jnp.einsum("qhd,kd->hqk", qr, k_rope[:end], preferred_element_type=f32)
        ) * scale
        q_seg = jnp.arange(begin, end) // SPAN
        k_seg = jnp.arange(end) // SPAN
        allowed = k_seg[None, :] <= q_seg[:, None]
        scores = jnp.where(allowed[None], scores, neg)
        probs = jax.nn.softmax(scores, axis=-1)
        d_probs = jnp.einsum("qhd,khd->hqk", go, values[:end], preferred_element_type=f32)
        d_scores = probs * (d_probs - jnp.sum(probs * d_probs, axis=-1, keepdims=True))
        ds_b = d_scores.astype(bf16)
        p_b = probs.astype(bf16)
        dq_n = jnp.einsum("hqk,khd->qhd", ds_b, key_nope[:end], preferred_element_type=f32) * scale
        dq_r = jnp.einsum("hqk,kd->qhd", ds_b, k_rope[:end], preferred_element_type=f32) * scale
        dq_r = rotate(dq_r, cosine[begin:end, None, :], -sine[begin:end, None, :])
        dq_parts.append(jnp.concatenate([dq_n, dq_r], axis=-1).astype(bf16))
        dk_nope = dk_nope.at[:end].add(
            jnp.einsum("hqk,qhd->khd", ds_b, qn, preferred_element_type=f32) * scale
        )
        dk_rope = dk_rope.at[:end].add(
            jnp.einsum("hqk,qhd->kd", ds_b, qr, preferred_element_type=f32) * scale
        )
        d_vals = d_vals.at[:end].add(
            jnp.einsum("hqk,qhd->khd", p_b, go, preferred_element_type=f32)
        )
    query_part = jnp.concatenate(dq_parts, axis=0)
    grads = jnp.concatenate([query_part, dk_nope.astype(bf16), d_vals.astype(bf16)], axis=-1)
    return (grads, rotate(dk_rope, cosine, -sine))


def local(query, latent, rope_key, latent_norm_gain, key_up_matrix, value_up_matrix, out_grad):
    f32 = jnp.float32
    bf16 = jnp.bfloat16
    tokens = latent.shape[1]
    width = PLAIN_HEAD_WIDTH + ROPE
    head_cols = ATTENTION_HEADS * PLAIN_HEAD_WIDTH
    lat = latent[0].astype(f32)
    inv_rms = lax.rsqrt(jnp.mean(lat * lat, axis=-1, keepdims=True) + eps)
    normed = lat * inv_rms
    nlat = (normed * latent_norm_gain).astype(bf16)
    stacked = jnp.stack([key_up_matrix, value_up_matrix])
    whole = lax.all_gather(stacked, "dp", axis=1, tiled=True)
    kv_tok = jnp.einsum("tc,gnc->tgn", nlat, whole, preferred_element_type=f32).astype(bf16)
    heads_query = query[0].reshape(tokens, ATTENTION_HEADS, width)
    key_nope = kv_tok[:, 0].reshape(tokens, ATTENTION_HEADS, PLAIN_HEAD_WIDTH)
    values = kv_tok[:, 1].reshape(tokens, ATTENTION_HEADS, VALUE_HEAD_WIDTH)
    d_out = out_grad[0].reshape(tokens, ATTENTION_HEADS, VALUE_HEAD_WIDTH)
    packed = jnp.concatenate([heads_query, key_nope, values, d_out], axis=2)
    arrived = lax.all_to_all(packed, "sp", split_axis=1, concat_axis=0, tiled=True)
    rope_full = lax.all_gather(rope_key[0], "sp", axis=0, tiled=True)
    grads_heads, rope_full_grad = attend_backward(arrived, rope_full)
    returned = lax.all_to_all(grads_heads, "sp", split_axis=0, concat_axis=1, tiled=True)
    rope_grad = lax.psum_scatter(rope_full_grad, "sp", scatter_dimension=0, tiled=True)
    query_grad = returned[:, :, :width].reshape(tokens, ATTENTION_HEADS * width)
    key_cols = returned[:, :, width : width + PLAIN_HEAD_WIDTH].reshape(tokens, head_cols)
    value_cols = returned[:, :, width + PLAIN_HEAD_WIDTH :].reshape(tokens, head_cols)
    dkv = jnp.stack([key_cols, value_cols], axis=1)
    d_nlat = jnp.einsum("tgn,gnc->tc", dkv, whole, preferred_element_type=f32)
    latents_all = lax.all_gather(nlat[None], "dp", axis=0, tiled=True)
    columns = lax.all_to_all(dkv[None], "dp", split_axis=3, concat_axis=0, tiled=True)
    partial_value = jnp.einsum("stgr,stc->grc", columns, latents_all, preferred_element_type=f32)
    weight_grads = lax.psum(partial_value, "sp")
    gain_grad = lax.psum(jnp.sum(d_nlat * normed, axis=0), ("sp", "dp"))
    scaled = d_nlat * latent_norm_gain
    latent_grad = inv_rms * (scaled - normed * jnp.mean(scaled * normed, axis=-1, keepdims=True))
    return (
        query_grad[None],
        latent_grad[None],
        rope_grad[None],
        weight_grads[0],
        weight_grads[1],
        gain_grad,
    )


def solution(mesh):
    in_specs = (
        P("dp", "sp", None),
        P("dp", "sp", None),
        P("dp", "sp", None),
        P(),
        P("dp", None),
        P("dp", None),
        P("dp", "sp", None),
    )
    out_specs = (
        P("dp", "sp", None),
        P("dp", "sp", None),
        P("dp", "sp", None),
        P("dp", None),
        P("dp", None),
        P(),
    )
    return jax.shard_map(local, mesh=mesh, in_specs=in_specs, out_specs=out_specs, check_vma=False)
```

profile of v0, /device:TPU:0, one launch (start us, length us, event | category | flops | bytes accessed | tf_op | source)
XLA Modules:
  0.0 738.0 jit_solution(6265751976223707838)
XLA Ops:
  16.4 55.1 %all-gather.4.cloned.1.call-done = bf16[2,2048,1024]{2,1,0:T(8,128)(2,1)} async-done(((bf16[2,512,1024]{2,1,0:T(8,128)(2,1)}), bf16[2,2048,1024]{2,1,0:T(8,128)(2,1)}) %all-gather.4.cloned.1.call-update) | async-done | bytes 8388624 | tf_op jit(solution)/shard_map/all_gather | solution.py:99
  71.5 6.2 convolution_convert_fusion
  87.8 5.6 pad_maximum_fusion
  93.4 4.0 copy.97
  97.4 5.6 all-to-all-start
  103.2 126.8 %all-gather = bf16[1,1536,32]{2,0,1:T(2,128)(2,1)S(1)} all-gather(bf16[1,192,32]{2,0,1:T(2,128)(2,1)S(1)} %copy.99), channel_id=2, replica_groups=mesh['sp'=8,'dp'=4] {'sp'}, dimensions={1}, use_global_device_ids=true | all-gather | bytes 110592 | tf_op jit(solution)/shard_map/all_gather | solution.py:107
  236.4 8.3 %copy.98 = bf16[8,192,4,288]{1,0,3,2:T(8,128)(2,1)} copy(bf16[8,192,4,288]{3,1,2,0:T(8,128)(2,1)} %bitcast.8) | data formatting | bytes 7077888 | tf_op jit(solution)/shard_map/all_to_all | solution.py:106
  244.7 6.9 all_to_all.42
  258.0 5.4 fusion.43
  283.7 9.7 %multiply_convert_fusion.1 = bf16[4,512,1024]{2,1,0:T(8,128)(2,1)S(1)} fusion(f32[4,512,1024]{2,1,0:T(8,128)S(1)} %get-tuple-element.177, f32[4,512]{1,0:T(4,128)S(1)} %get-tuple-element.176, f32[4,512,1024]{2,1,0:T(8,128)S(1)} %get-tuple-element.171, f32[4,512]{1,0:T(4,128)S(1)} %get-tuple-element.170), kind=kLoop, calls=%fused_computation.12 | loop fusion | flops 8388608 | bytes 20987904 | tf_op jit(solution)/shard_map/convert_element_type | solution.py:68
  300.5 8.5 %fusion.4 = f32[4,512,1536]{2,1,0:T(8,128)} fusion(f32[1536,512,4]{0,1,2:T(8,128)S(1)} %fusion.114, pred[512,1536]{1,0:T(8,128)(4,1)S(1)} %copy-done.13, bf16[1536,4,288]{0,2,1:T(8,128)(2,1)} %copy-done.3), kind=kOutput, calls=%fused_computation.5 | convolution fusion | flops 412090368 | bytes 27000832 | tf_op jit(solution)/shard_map/qhd,khd->hqk/dot_general | solution.py:57
  309.1 14.9 %fusion.154 = (f32[4,512]{1,0:T(4,128)S(1)}, f32[4,512,1536]{2,1,0:T(8,128)}) fusion(f32[4,512,1536]{2,1,0:T(8,128)} %fusion.4), kind=kOutput, calls=%fused_computation.226 | output fusion | flops 6292991 | bytes 25174016 | tf_op jit(solution)/shard_map/sub | solution.py:65
  323.9 11.8 %multiply_reduce_fusion = (f32[4,512]{1,0:T(4,128)S(1)}, f32[4,512,1536]{2,1,0:T(8,128)}) fusion(f32[4,512,1536]{2,1,0:T(8,128)} %get-tuple-element.173, f32[4,512]{1,0:T(4,128)S(1)} %get-tuple-element.172, bf16[1536,4,288]{0,2,1:T(8,128)(2,1)} %copy-done.3), kind=kOutput, calls=%fused_computation.7 | convolution fusion | flops 412088320 | bytes 26230784 | tf_op jit(solution)/shard_map/qhd,khd->hqk/dot_general | solution.py:66
  335.7 6.0 multiply_convert_fusion
  341.8 4.5 fusion.52
  351.6 11.2 %fusion.37 = f32[1536,4,64]{0,2,1:T(8,128)} fusion(f32[1536,4,64]{0,2,1:T(8,128)} %scatter-add.24, bf16[1536,4,288]{0,2,1:T(8,128)(2,1)} %copy-done.3, f32[4,512]{1,0:T(4,128)S(1)} %get-tuple-element.170, f32[4,512,1024]{2,1,0:T(8,128)} %copy-done.2), kind=kOutput, calls=%fused_computation.53 | convolution fusion | flops 274992128 | bytes 19144704 | tf_op jit(solution)/shard_map/hqk,qhd->khd/dot_general | solution.py:81
  362.8 4.4 fusion.42
  367.2 13.7 %fusion.22 = bf16[1536,4,64]{0,2,1:T(8,128)(2,1)} fusion(f32[1536,4,64]{0,2,1:T(8,128)} %fusion.37, bf16[1536,4,288]{0,2,1:T(8,128)(2,1)} %copy-done.3, f32[4,512]{1,0:T(4,128)S(1)} %get-tuple-element.172, f32[4,512,1536]{2,1,0:T(8,128)} %fusion.4), kind=kOutput, calls=%fused_computation.36 | convolution fusion | flops 412880384 | bytes 27795456 | tf_op jit(solution)/shard_map/hqk,qhd->khd/dot_general | solution.py:81
  381.0 4.6 fusion.21
  388.8 5.8 copy.107
  394.6 4.6 all-to-all-start.1
  401.9 64.4 %all-to-all-done.1 = bf16[1536,4,224]{2,1,0:T(4,128)(2,1)} async-done(((bf16[1536,4,224]{2,1,0:T(4,128)(2,1)}), bf16[1536,4,224]{2,1,0:T(4,128)(2,1)}, u32[]{:S(2)}, u32[]{:S(2)}) %all-to-all-start.1) | async-done | bytes 2752544 | tf_op jit(solution)/shard_map/all_to_all | solution.py:109
  483.8 6.1 copy.116
  489.8 4.4 all-to-all-start.2
  503.7 16.3 %all-to-all-done.2 = bf16[1,192,2,2048]{1,2,0,3:T(2,128)(2,1)} async-done(((bf16[1,192,2,2048]{1,2,0,3:T(2,128)(2,1)}), bf16[1,192,2,2048]{1,2,0,3:T(2,128)(2,1)}, u32[]{:S(2)}, u32[]{:S(2)}) %all-to-all-start.2) | async-done | bytes 1572896 | tf_op jit(solution)/shard_map/all_to_all | solution.py:117
  520.0 6.0 copy.118
  526.0 5.7 convolution_bitcast_fusion.1
  531.7 34.6 %reduce-scatter.4.cloned.1.call-done = f32[192,32]{1,0:T(8,128)} async-done(((f32[1536,32]{1,0:T(8,128)}), f32[192,32]{1,0:T(8,128)}) %reduce-scatter.4.cloned.1.call-update) | async-done | bytes 24592
  572.2 6.3 fusion.72
  578.5 44.0 %psum.15 = f32[1024]{0:T(1024)} all-reduce(f32[1024]{0:T(1024)S(1)} %get-tuple-element.138), channel_id=1, replica_groups=mesh['sp'=8,'dp'=4] {'sp','dp'}, use_global_device_ids=true, to_apply=%region_14.15 | all-reduce | flops 1024 | bytes 8192 | tf_op jit(solution)/shard_map/psum | solution.py:120
  623.6 102.6 %all-reduce.5.cloned.1.call-done = f32[2,512,1024]{2,1,0:T(8,128)} async-done(((f32[2,512,1024]{2,1,0:T(8,128)}), f32[2,512,1024]{2,1,0:T(8,128)}) %all-reduce.5.cloned.1.call-update) | async-done | bytes 4194320 | tf_op jit(solution)/shard_map/psum | solution.py:119
  726.2 4.8 slice_bitcast_fusion
  (184 shorter events, 104.2 us)
Async XLA Ops:
  7.2 64.3 %all-gather.4.cloned.1.call-start = ((), (), s32[]{:S(2)}) async-start(), calls=%async_computation.4 | async-start | bytes 10485760 | tf_op jit(solution)/shard_map/all_gather | solution.py:99
  10.3 5.9 copy-start.10
  10.4 61.1 %copy-start.41 = (f32[1024]{0:T(1024)S(1)}, f32[1024]{0:T(1024)}, u32[]{:S(2)}) copy-start(f32[1024]{0:T(1024)} %param.34) | copy-start | bytes 12292
  16.4 55.1 %copy-start.44 = (f32[192]{0:T(256)}, f32[192]{0:T(256)S(1)}, u32[]{:S(2)}) copy-start(f32[192]{0:T(256)S(1)} %add_rsqrt_fusion) | copy-start | bytes 2308
  97.4 5.7 copy-start.43
  97.4 139.0 %all-to-all-start = ((bf16[192,32,288]{2,0,1:T(8,128)(2,1)}), bf16[192,32,288]{2,0,1:T(8,128)(2,1)}, u32[]{:S(2)}, u32[]{:S(2)}) async-start(bf16[192,32,288]{2,0,1:T(8,128)(2,1)} %copy.97), calls=%async_computation | async-start | bytes 9437184 | tf_op jit(solution)/shard_map/all_to_all | solution.py:106
  251.6 11.8 %copy-start.3 = (bf16[1536,4,288]{0,2,1:T(8,128)(2,1)}, bf16[1536,4,288]{0,2,1:T(8,128)(2,1)S(1)}, u32[]{:S(2)}) copy-start(bf16[1536,4,288]{0,2,1:T(8,128)(2,1)S(1)} %all_to_all.42) | copy-start | bytes 10616836
  268.0 5.0 copy-start.7
  268.0 5.0 copy-start.9
  293.4 5.2 copy-start.1
  323.9 11.8 %slice-start = ((s8[12582912]{0:T(1024)(128)(4,1)}), s8[4194304]{0:T(1024)(128)(4,1)S(1)}, s32[]{:S(2)}) async-start(s8[12582912]{0:T(1024)(128)(4,1)} %bitcast.187), calls=%async_computation.8 | async-start | bytes 8388608
  323.9 11.8 %slice-start.1 = ((s8[12582912]{0:T(1024)(128)(4,1)}), s8[4194304]{0:T(1024)(128)(4,1)S(1)}, s32[]{:S(2)}) async-start(s8[12582912]{0:T(1024)(128)(4,1)} %bitcast.187), calls=%async_computation.9 | async-start | bytes 8388608
  323.9 11.8 %slice-start.2 = ((s8[12582912]{0:T(1024)(128)(4,1)}), s8[4194304]{0:T(1024)(128)(4,1)S(1)}, s32[]{:S(2)}) async-start(s8[12582912]{0:T(1024)(128)(4,1)} %bitcast.187), calls=%async_computation.10 | async-start | bytes 8388608
  341.8 7.1 copy-start
  380.9 4.8 copy-start.22
  380.9 4.8 copy-start.37
  380.9 4.8 copy-start.38
  380.9 4.9 copy-start.23
  380.9 4.9 copy-start.35
  380.9 4.9 copy-start.36
  380.9 4.9 copy-start.25
  381.0 4.9 copy-start.26
  381.0 4.9 copy-start.27
  381.0 4.9 copy-start.33
  394.6 4.9 copy-start.11
  394.6 4.9 copy-start.42
  394.6 4.9 copy-start.45
  394.6 71.6 %all-to-all-start.1 = ((bf16[1536,4,224]{2,1,0:T(4,128)(2,1)}), bf16[1536,4,224]{2,1,0:T(4,128)(2,1)}, u32[]{:S(2)}, u32[]{:S(2)}) async-start(bf16[1536,4,224]{2,1,0:T(4,128)(2,1)} %copy.107), calls=%async_computation.1 | async-start | bytes 6291456 | tf_op jit(solution)/shard_map/all_to_all | solution.py:109
  399.2 126.8 %all-gather.6.cloned.1.call-start = ((), (), s32[]{:S(2)}) async-start(), calls=%async_computation.5 | async-start | bytes 1966080 | tf_op jit(solution)/shard_map/all_gather | solution.py:116
  489.8 30.2 %all-to-all-start.2 = ((bf16[1,192,2,2048]{1,2,0,3:T(2,128)(2,1)}), bf16[1,192,2,2048]{1,2,0,3:T(2,128)(2,1)}, u32[]{:S(2)}, u32[]{:S(2)}) async-start(bf16[1,192,2,2048]{1,2,0,3:T(2,128)(2,1)} %copy.116), calls=%async_computation.2 | async-start | bytes 4194304 | tf_op jit(solution)/shard_map/all_to_all | solution.py:117
  494.3 72.0 %reduce-scatter.4.cloned.1.call-start = ((), (), s32[]{:S(2)}) async-start(), calls=%async_computation.7 | async-start | bytes 884736
  503.6 222.6 %all-reduce.5.cloned.1.call-start = ((), (), s32[]{:S(2)}) async-start(), calls=%async_computation.6 | async-start | bytes 8388608 | tf_op jit(solution)/shard_map/psum | solution.py:119
  (26 other events, 64.0 us)
Sparse Core Ops, SparseCore 0:
  10.5 60.9 all-gather.3
  401.6 19.9 all-gather.5
  503.8 62.4 reduce-scatter.3
  569.8 156.3 all-reduce.4
where the time goes:
time: 747 us; the launch traced here: 738 us
  waiting for transfers between devices  273 us (37%)
  blocking collectives  171 us (23%)
  matrix products  118 us (16%)
  local copies, waits for them, and re-layouts  87 us (12%)
  other arithmetic  59.6 us (8%)
  starting transfers between devices  15.1 us (2%)
  between operations  15 us (2%)
    all_gather x1, blocking collectives, local(): rope_full = lax.all_gather(rope_key[0], 'sp', axis=0, tiled=True)  127 us
    psum x1, waiting for transfers between devices, local(): weight_grads = lax.psum(partial_value, 'sp')  103 us
    all_to_all x1, waiting for transfers between devices, local(): lax.all_to_all(grads_heads, 'sp', split_axis=0, concat_axis=1, tiled=True)  64.4 us
    all_gather x1, waiting for transfers between devices, local(): whole = lax.all_gather(stacked, 'dp', axis=1, tiled=True)  55.1 us
    psum x1, blocking collectives, local(): gain_grad = lax.psum(jnp.sum(d_nlat * normed, axis=0), ('sp', 'dp'))  44 us
    unnamed x5, waiting for transfers between devices  34.6 us
    dot_general x3, matrix products, attend_backward(): jnp.einsum('hqk,qhd->khd', p_b, go, preferred_element_type=f32)  30.3 us
    sub x3, other arithmetic, attend_backward(): probs = jax.nn.softmax(scores, axis=-1)  20.1 us
  transfers between devices with their start and end apart: 7, of which 5 were waited for; matrix products, arithmetic and copies ran while one was open for 10% of the time, Pallas kernels for 0%

commit v1 on v0

--- a/solution.py
+++ b/solution.py
@@ -117,7 +117,9 @@
     columns = lax.all_to_all(dkv[None], "dp", split_axis=3, concat_axis=0, tiled=True)
     partial_value = jnp.einsum("stgr,stc->grc", columns, latents_all, preferred_element_type=f32)
     weight_grads = lax.psum(partial_value, "sp")
-    gain_grad = lax.psum(jnp.sum(d_nlat * normed, axis=0), ("sp", "dp"))
+    gain_grad = jnp.sum(d_nlat * normed, axis=0)
+    for over in ("dp", "sp"):
+        gain_grad = lax.psum(gain_grad, over)
     scaled = d_nlat * latent_norm_gain
     latent_grad = inv_rms * (scaled - normed * jnp.mean(scaled * normed, axis=-1, keepdims=True))
     return (

time: 747 us -> 747 us (level)
  blocking collectives: 171 us -> 153 us
  waiting for transfers between devices: 273 us -> 290 us
    psum x1 -> x2, blocking collectives: 44 us -> 26.1 us  [local(): gain_grad = lax.psum(gain_grad, over)]
    psum x1, waiting for transfers between devices: 103 us -> 120 us  [local(): weight_grads = lax.psum(partial_value, 'sp')]
where the time goes in v1:
time: 747 us; the launch traced here: 738 us
  waiting for transfers between devices  290 us (39%)
  blocking collectives  153 us (20%)
  matrix products  118 us (16%)
  local copies, waits for them, and re-layouts  87 us (12%)
  other arithmetic  59.7 us (8%)
  starting transfers between devices  15.1 us (2%)
  between operations  15 us (2%)
    all_gather x1, blocking collectives, local(): rope_full = lax.all_gather(rope_key[0], 'sp', axis=0, tiled=True)  127 us
    psum x1, waiting for transfers between devices, local(): weight_grads = lax.psum(partial_value, 'sp')  120 us
    all_to_all x1, waiting for transfers between devices, local(): lax.all_to_all(grads_heads, 'sp', split_axis=0, concat_axis=1, tiled=True)  64.4 us
    all_gather x1, waiting for transfers between devices, local(): whole = lax.all_gather(stacked, 'dp', axis=1, tiled=True)  55.1 us
    unnamed x5, waiting for transfers between devices  34.6 us
    dot_general x3, matrix products, attend_backward(): jnp.einsum('hqk,qhd->khd', p_b, go, preferred_element_type=f32)  30.4 us
    psum x2, blocking collectives, local(): gain_grad = lax.psum(gain_grad, over)  26.1 us
    sub x3, other arithmetic, attend_backward(): probs = jax.nn.softmax(scores, axis=-1)  20.1 us
  transfers between devices with their start and end apart: 7, of which 5 were waited for; matrix products, arithmetic and copies ran while one was open for 10% of the time, Pallas kernels for 0%

profile of v1, /device:TPU:0, one launch (start us, length us, event | category | flops | bytes accessed | tf_op | source)
XLA Modules:
  0.0 737.5 jit_solution(2584245670333585449)
XLA Ops:
  16.4 55.1 %all-gather.4.cloned.1.call-done = bf16[2,2048,1024]{2,1,0:T(8,128)(2,1)} async-done(((bf16[2,512,1024]{2,1,0:T(8,128)(2,1)}), bf16[2,2048,1024]{2,1,0:T(8,128)(2,1)}) %all-gather.4.cloned.1.call-update) | async-done | bytes 8388624 | tf_op jit(solution)/shard_map/all_gather | solution.py:99
  71.5 6.2 convolution_convert_fusion
  87.8 5.6 pad_maximum_fusion
  97.4 5.6 all-to-all-start
  103.1 126.8 %all-gather = bf16[1,1536,32]{2,0,1:T(2,128)(2,1)S(1)} all-gather(bf16[1,192,32]{2,0,1:T(2,128)(2,1)S(1)} %copy.99), channel_id=2, replica_groups=mesh['sp'=8,'dp'=4] {'sp'}, dimensions={1}, use_global_device_ids=true | all-gather | bytes 110592 | tf_op jit(solution)/shard_map/all_gather | solution.py:107
  236.4 8.3 %copy.98 = bf16[8,192,4,288]{1,0,3,2:T(8,128)(2,1)} copy(bf16[8,192,4,288]{3,1,2,0:T(8,128)(2,1)} %bitcast.8) | data formatting | bytes 7077888 | tf_op jit(solution)/shard_map/all_to_all | solution.py:106
  244.7 6.9 all_to_all.42
  257.9 5.4 fusion.43
  283.6 9.7 %multiply_convert_fusion.1 = bf16[4,512,1024]{2,1,0:T(8,128)(2,1)S(1)} fusion(f32[4,512,1024]{2,1,0:T(8,128)S(1)} %get-tuple-element.177, f32[4,512]{1,0:T(4,128)S(1)} %get-tuple-element.176, f32[4,512,1024]{2,1,0:T(8,128)S(1)} %get-tuple-element.171, f32[4,512]{1,0:T(4,128)S(1)} %get-tuple-element.170), kind=kLoop, calls=%fused_computation.12 | loop fusion | flops 8388608 | bytes 20987904 | tf_op jit(solution)/shard_map/convert_element_type | solution.py:68
  300.5 8.5 %fusion.4 = f32[4,512,1536]{2,1,0:T(8,128)} fusion(f32[1536,512,4]{0,1,2:T(8,128)S(1)} %fusion.114, pred[512,1536]{1,0:T(8,128)(4,1)S(1)} %copy-done.13, bf16[1536,4,288]{0,2,1:T(8,128)(2,1)} %copy-done.3), kind=kOutput, calls=%fused_computation.5 | convolution fusion | flops 412090368 | bytes 27000832 | tf_op jit(solution)/shard_map/qhd,khd->hqk/dot_general | solution.py:57
  309.0 14.9 %fusion.154 = (f32[4,512]{1,0:T(4,128)S(1)}, f32[4,512,1536]{2,1,0:T(8,128)}) fusion(f32[4,512,1536]{2,1,0:T(8,128)} %fusion.4), kind=kOutput, calls=%fused_computation.226 | output fusion | flops 6292991 | bytes 25174016 | tf_op jit(solution)/shard_map/sub | solution.py:65
  323.9 11.8 %multiply_reduce_fusion = (f32[4,512]{1,0:T(4,128)S(1)}, f32[4,512,1536]{2,1,0:T(8,128)}) fusion(f32[4,512,1536]{2,1,0:T(8,128)} %get-tuple-element.173, f32[4,512]{1,0:T(4,128)S(1)} %get-tuple-element.172, bf16[1536,4,288]{0,2,1:T(8,128)(2,1)} %copy-done.3), kind=kOutput, calls=%fused_computation.7 | convolution fusion | flops 412088320 | bytes 26230784 | tf_op jit(solution)/shard_map/qhd,khd->hqk/dot_general | solution.py:66
  335.7 6.0 multiply_convert_fusion
  341.8 4.5 fusion.52
  351.6 11.2 %fusion.37 = f32[1536,4,64]{0,2,1:T(8,128)} fusion(f32[1536,4,64]{0,2,1:T(8,128)} %scatter-add.24, bf16[1536,4,288]{0,2,1:T(8,128)(2,1)} %copy-done.3, f32[4,512]{1,0:T(4,128)S(1)} %get-tuple-element.170, f32[4,512,1024]{2,1,0:T(8,128)} %copy-done.2), kind=kOutput, calls=%fused_computation.53 | convolution fusion | flops 274992128 | bytes 19144704 | tf_op jit(solution)/shard_map/hqk,qhd->khd/dot_general | solution.py:81
  362.8 4.4 fusion.42
  367.2 13.7 %fusion.22 = bf16[1536,4,64]{0,2,1:T(8,128)(2,1)} fusion(f32[1536,4,64]{0,2,1:T(8,128)} %fusion.37, bf16[1536,4,288]{0,2,1:T(8,128)(2,1)} %copy-done.3, f32[4,512]{1,0:T(4,128)S(1)} %get-tuple-element.172, f32[4,512,1536]{2,1,0:T(8,128)} %fusion.4), kind=kOutput, calls=%fused_computation.36 | convolution fusion | flops 412880384 | bytes 27795456 | tf_op jit(solution)/shard_map/hqk,qhd->khd/dot_general | solution.py:81
  381.1 4.6 fusion.21
  388.9 5.8 copy.107
  394.7 4.6 all-to-all-start.1
  402.1 64.4 %all-to-all-done.1 = bf16[1536,4,224]{2,1,0:T(4,128)(2,1)} async-done(((bf16[1536,4,224]{2,1,0:T(4,128)(2,1)}), bf16[1536,4,224]{2,1,0:T(4,128)(2,1)}, u32[]{:S(2)}, u32[]{:S(2)}) %all-to-all-start.1) | async-done | bytes 2752544 | tf_op jit(solution)/shard_map/all_to_all | solution.py:109
  483.9 6.1 copy.116
  490.0 4.4 all-to-all-start.2
  503.9 16.3 %all-to-all-done.2 = bf16[1,192,2,2048]{1,2,0,3:T(2,128)(2,1)} async-done(((bf16[1,192,2,2048]{1,2,0,3:T(2,128)(2,1)}), bf16[1,192,2,2048]{1,2,0,3:T(2,128)(2,1)}, u32[]{:S(2)}, u32[]{:S(2)}) %all-to-all-start.2) | async-done | bytes 1572896 | tf_op jit(solution)/shard_map/all_to_all | solution.py:117
  520.2 6.0 copy.118
  526.2 5.7 convolution_bitcast_fusion.1
  531.9 34.6 %reduce-scatter.4.cloned.1.call-done = f32[192,32]{1,0:T(8,128)} async-done(((f32[1536,32]{1,0:T(8,128)}), f32[192,32]{1,0:T(8,128)}) %reduce-scatter.4.cloned.1.call-update) | async-done | bytes 24592
  572.4 6.3 fusion.72
  578.7 6.1 psum.22
  584.8 20.0 %psum.23 = f32[1024]{0:T(1024)} all-reduce(f32[1024]{0:T(1024)S(1)} %psum.22), channel_id=1, replica_groups=mesh['sp'=8,'dp'=4] {'sp'}, use_global_device_ids=true, to_apply=%region_15.16 | all-reduce | flops 1024 | bytes 8192 | tf_op jit(solution)/shard_map/psum | solution.py:122
  605.9 119.8 %all-reduce.5.cloned.1.call-done = f32[2,512,1024]{2,1,0:T(8,128)} async-done(((f32[2,512,1024]{2,1,0:T(8,128)}), f32[2,512,1024]{2,1,0:T(8,128)}) %all-reduce.5.cloned.1.call-update) | async-done | bytes 4194320 | tf_op jit(solution)/shard_map/psum | solution.py:119
  725.7 4.8 slice_bitcast_fusion
  (185 shorter events, 108.2 us)
Async XLA Ops:
  7.2 64.3 %all-gather.4.cloned.1.call-start = ((), (), s32[]{:S(2)}) async-start(), calls=%async_computation.4 | async-start | bytes 10485760 | tf_op jit(solution)/shard_map/all_gather | solution.py:99
  10.3 5.9 copy-start.10
  10.4 61.1 %copy-start.41 = (f32[1024]{0:T(1024)S(1)}, f32[1024]{0:T(1024)}, u32[]{:S(2)}) copy-start(f32[1024]{0:T(1024)} %param.34) | copy-start | bytes 12292
  16.4 55.1 %copy-start.44 = (f32[192]{0:T(256)}, f32[192]{0:T(256)S(1)}, u32[]{:S(2)}) copy-start(f32[192]{0:T(256)S(1)} %add_rsqrt_fusion) | copy-start | bytes 2308
  97.4 5.7 copy-start.43
  97.4 139.0 %all-to-all-start = ((bf16[192,32,288]{2,0,1:T(8,128)(2,1)}), bf16[192,32,288]{2,0,1:T(8,128)(2,1)}, u32[]{:S(2)}, u32[]{:S(2)}) async-start(bf16[192,32,288]{2,0,1:T(8,128)(2,1)} %copy.97), calls=%async_computation | async-start | bytes 9437184 | tf_op jit(solution)/shard_map/all_to_all | solution.py:106
  251.6 11.7 %copy-start.3 = (bf16[1536,4,288]{0,2,1:T(8,128)(2,1)}, bf16[1536,4,288]{0,2,1:T(8,128)(2,1)S(1)}, u32[]{:S(2)}) copy-start(bf16[1536,4,288]{0,2,1:T(8,128)(2,1)S(1)} %all_to_all.42) | copy-start | bytes 10616836
  268.0 5.0 copy-start.7
  268.0 5.0 copy-start.9
  293.4 5.3 copy-start.1
  323.9 11.8 %slice-start = ((s8[12582912]{0:T(1024)(128)(4,1)}), s8[4194304]{0:T(1024)(128)(4,1)S(1)}, s32[]{:S(2)}) async-start(s8[12582912]{0:T(1024)(128)(4,1)} %bitcast.187), calls=%async_computation.8 | async-start | bytes 8388608
  323.9 11.8 %slice-start.1 = ((s8[12582912]{0:T(1024)(128)(4,1)}), s8[4194304]{0:T(1024)(128)(4,1)S(1)}, s32[]{:S(2)}) async-start(s8[12582912]{0:T(1024)(128)(4,1)} %bitcast.187), calls=%async_computation.9 | async-start | bytes 8388608
  323.9 11.8 %slice-start.2 = ((s8[12582912]{0:T(1024)(128)(4,1)}), s8[4194304]{0:T(1024)(128)(4,1)S(1)}, s32[]{:S(2)}) async-start(s8[12582912]{0:T(1024)(128)(4,1)} %bitcast.187), calls=%async_computation.10 | async-start | bytes 8388608
  341.8 7.2 copy-start
  381.0 4.8 copy-start.22
  381.0 4.8 copy-start.37
  381.0 4.8 copy-start.38
  381.0 4.9 copy-start.23
  381.0 4.9 copy-start.35
  381.0 4.9 copy-start.36
  381.0 4.9 copy-start.25
  381.0 4.9 copy-start.26
  381.1 4.9 copy-start.27
  381.1 4.9 copy-start.33
  394.7 4.9 copy-start.11
  394.7 4.9 copy-start.42
  394.7 4.9 copy-start.45
  394.7 71.7 %all-to-all-start.1 = ((bf16[1536,4,224]{2,1,0:T(4,128)(2,1)}), bf16[1536,4,224]{2,1,0:T(4,128)(2,1)}, u32[]{:S(2)}, u32[]{:S(2)}) async-start(bf16[1536,4,224]{2,1,0:T(4,128)(2,1)} %copy.107), calls=%async_computation.1 | async-start | bytes 6291456 | tf_op jit(solution)/shard_map/all_to_all | solution.py:109
  399.3 126.9 %all-gather.6.cloned.1.call-start = ((), (), s32[]{:S(2)}) async-start(), calls=%async_computation.5 | async-start | bytes 1966080 | tf_op jit(solution)/shard_map/all_gather | solution.py:116
  490.0 30.2 %all-to-all-start.2 = ((bf16[1,192,2,2048]{1,2,0,3:T(2,128)(2,1)}), bf16[1,192,2,2048]{1,2,0,3:T(2,128)(2,1)}, u32[]{:S(2)}, u32[]{:S(2)}) async-start(bf16[1,192,2,2048]{1,2,0,3:T(2,128)(2,1)} %copy.116), calls=%async_computation.2 | async-start | bytes 4194304 | tf_op jit(solution)/shard_map/all_to_all | solution.py:117
  494.4 72.0 %reduce-scatter.4.cloned.1.call-start = ((), (), s32[]{:S(2)}) async-start(), calls=%async_computation.7 | async-start | bytes 884736
  503.8 221.9 %all-reduce.5.cloned.1.call-start = ((), (), s32[]{:S(2)}) async-start(), calls=%async_computation.6 | async-start | bytes 8388608 | tf_op jit(solution)/shard_map/psum | solution.py:119
  (26 other events, 64.0 us)
Sparse Core Ops, SparseCore 0:
  10.5 60.9 all-gather.3
  401.7 19.9 all-gather.5
  503.9 62.4 reduce-scatter.3
  570.0 155.6 all-reduce.4
